TPU v7x, 32 devices: a whole 2x2x4 slice. The times are simulated.
32 devices in a mesh: fs: 8 (over z, core), tp: 4 (over y, x).
Axes of the slice: x: 2, y: 2, z: 4, core: 2. Of those that a mesh axis runs over, the one named last changes fastest.
Arguments:
- saved_input: bfloat16 [6144, 2048], P('fs'), may hold values from -6 to 6
- query_cot: bfloat16 [6144, 2048], P('fs', 'tp'), may hold values from -120 to 120
- head_out: bfloat16 [6144, 2048], P('fs', 'tp'), may hold values from -120 to 120
- output_cot: bfloat16 [6144, 2048], P('fs'), may hold values from -6 to 6
- basis_q: bfloat16 [2048, 128], replicated, may hold values from -0.125 to 0.125
- basis_o: bfloat16 [2048, 128], replicated, may hold values from -0.125 to 0.125
- weight_q: float32 [2048, 2048], P('fs', 'tp'), may hold values from -0.125 to 0.125
- weight_o: float32 [2048, 2048], P('tp', 'fs'), may hold values from -0.125 to 0.125
- first_q: float32 [128, 2048], P(None, 'tp'), may hold values from -2 to 2
- second_q: float32 [128, 2048], P(None, 'tp'), may hold values from 0.01 to 1
- first_o: float32 [2048, 128], P('tp'), may hold values from -2 to 2
- second_o: float32 [2048, 128], P('tp'), may hold values from 0.01 to 1
Outputs:
- step_q: float32 [2048, 2048], P('fs', 'tp')
- step_o: float32 [2048, 2048], P('tp', 'fs')
- new_weight_q: float32 [2048, 2048], P('fs', 'tp')
- new_weight_o: float32 [2048, 2048], P('tp', 'fs')
- copy_q: bfloat16 [2048, 2048], P(None, 'tp')
- copy_o: bfloat16 [2048, 2048], P('tp')
- moment_q: float32 [128, 2048], P(None, 'tp')
- square_q: float32 [128, 2048], P(None, 'tp')
- moment_o: float32 [2048, 128], P('tp')
- square_o: float32 [2048, 128], P('tp')
All inputs are finite; a program needn't handle non-finite values.
Results may differ from a plain program's by a relative error of at most 0.0035.
Values may be sent and summed in bfloat16 or wider, within the bound.
A program may use at most 64 MiB of HBM per device.

v0:
```python
import jax
import jax.numpy as jnp
from jax import lax
from jax.sharding import PartitionSpec as P

HEADS = 16
HEAD = 128
RANK = 128


BETA_FIRST = 0.9
BETA_SECOND = 0.95
ADAM_EPS = 1e-08
NORM_EPS = 1e-06
CLIP_RMS = 1.0
LEARN_RATE = 0.01


def split_product(factor_part, data_part):
    upper = factor_part.astype(jnp.bfloat16)
    lower = (factor_part - upper.astype(jnp.float32)).astype(jnp.bfloat16)
    first = jnp.dot(upper, data_part, preferred_element_type=jnp.float32)
    return first + jnp.dot(lower, data_part, preferred_element_type=jnp.float32)


def shards(
    saved_input,
    query_cot,
    head_out,
    output_cot,
    basis_q,
    basis_o,
    weight_q,
    weight_o,
    first_q,
    second_q,
    first_o,
    second_o,
):
    highest = lax.Precision.HIGHEST
    row_count = weight_q.shape[0]
    offset = lax.axis_index("fs") * row_count
    rows_q = lax.dynamic_slice_in_dim(basis_q, offset, row_count, 0).astype(jnp.float32)
    rows_o = lax.dynamic_slice_in_dim(basis_o, offset, row_count, 0).astype(jnp.float32)
    input_low = jnp.dot(saved_input, basis_q, preferred_element_type=jnp.float32)
    partial_q = split_product(input_low.T, query_cot)
    cot_low = jnp.dot(output_cot, basis_o, preferred_element_type=jnp.float32)
    partial_o = split_product(cot_low.T, head_out).T
    low_q, low_o = lax.psum((partial_q, partial_o), "fs")
    sum_q, sum_o = lax.psum((jnp.sum(low_q * low_q), jnp.sum(low_o * low_o)), "tp")
    rms_value = jnp.sqrt((sum_q + sum_o) / (2 * RANK * HEADS * HEAD) + NORM_EPS)
    factor = jnp.minimum(1.0, CLIP_RMS / rms_value)
    moment_q = BETA_FIRST * first_q + (1.0 - BETA_FIRST) * factor * low_q
    square_q = BETA_SECOND * second_q + (1.0 - BETA_SECOND) * (factor * low_q) ** 2
    moment_o = BETA_FIRST * first_o + (1.0 - BETA_FIRST) * factor * low_o
    square_o = BETA_SECOND * second_o + (1.0 - BETA_SECOND) * (factor * low_o) ** 2
    dir_q = moment_q / (jnp.sqrt(square_q) + ADAM_EPS)
    dir_o = moment_o / (jnp.sqrt(square_o) + ADAM_EPS)
    step_q = jnp.dot(rows_q, dir_q, precision=highest)
    step_o = jnp.dot(dir_o, rows_o.T, precision=highest)
    new_weight_q = weight_q - LEARN_RATE * step_q
    new_weight_o = weight_o - LEARN_RATE * step_o
    copy_q, copy_o = (
        lax.all_gather(new_weight_q.astype(jnp.bfloat16), "fs", axis=0, tiled=True),
        lax.all_gather(new_weight_o.astype(jnp.bfloat16), "fs", axis=1, tiled=True),
    )
    return (
        step_q,
        step_o,
        new_weight_q,
        new_weight_o,
        copy_q,
        copy_o,
        moment_q,
        square_q,
        moment_o,
        square_o,
    )


def solution(mesh):
    return jax.shard_map(
        shards,
        mesh=mesh,
        in_specs=(
            P("fs", None),
            P("fs", "tp"),
            P("fs", "tp"),
            P("fs", None),
            P(),
            P(),
            P("fs", "tp"),
            P("tp", "fs"),
            P(None, "tp"),
            P(None, "tp"),
            P("tp", None),
            P("tp", None),
        ),
        out_specs=(
            P("fs", "tp"),
            P("tp", "fs"),
            P("fs", "tp"),
            P("tp", "fs"),
            P(None, "tp"),
            P("tp", None),
            P(None, "tp"),
            P(None, "tp"),
            P("tp", None),
            P("tp", None),
        ),
        check_vma=False,
    )
```

profile of v0, /device:TPU:0, one launch (start us, length us, event | category | flops | bytes accessed | tf_op | source)
XLA Modules:
  0.0 164.3 jit_solution(583530073985837648)
XLA Ops:
  7.2 0.0 copy-start
  7.2 0.0 all-reduce.3.cloned.1.call-start
  7.2 1.8 %copy-done = bf16[768,2048]{1,0:T(8,128)(2,1)S(1)} copy-done((bf16[768,2048]{1,0:T(8,128)(2,1)S(1)}, bf16[768,2048]{1,0:T(8,128)(2,1)}, u32[]{:S(2)}) %copy-start) | copy-done | bytes 3145752
  9.1 2.4 %fusion.25 = f32[128,768]{1,0:T(8,128)S(1)} fusion(bf16[2048,128]{1,0:T(8,128)(2,1)} %param.16, bf16[768,2048]{1,0:T(8,128)(2,1)S(1)} %copy-done), kind=kOutput, calls=%fused_computation.37 | convolution fusion | flops 402653184 | bytes 4063232 | tf_op jit(solution)/shard_map/dot_general | solution.py:45
  11.5 0.3 fusion.15
  11.7 1.0 convolution_add_fusion.1
  12.7 1.2 fusion.26
  13.9 0.3 fusion.12
  14.2 1.0 fusion
  15.2 0.0 all-reduce.3.cloned.1.call-update
  15.2 0.0 all-gather.5.cloned.1.call-start
  15.2 0.8 copy.22
  16.1 1.8 %copy.23 = f32[512,128]{0,1:T(8,128)} copy(f32[512,128]{1,0:T(8,128)} %param.23) | data formatting | bytes 524288 | tf_op args[11]
  17.9 56.8 %all-reduce.3.cloned.1.call-done = (f32[128,512]{1,0:T(8,128)}, f32[512,128]{0,1:T(8,128)}) async-done(((f32[128,512]{1,0:T(8,128)}, f32[512,128]{0,1:T(8,128)}), (f32[128,512]{1,0:T(8,128)}, f32[512,128]{0,1:T(8,128)})) %all-reduce.3.cloned.1.call-update) | async-done | bytes 524304 | tf_op jit(solution)/shard_map/psum | solution.py:49
  74.7 1.6 multiply_reduce_fusion
  76.3 1.6 multiply_reduce_fusion.1
  79.2 10.3 %psum.32 = f32[]{:T(128)} all-reduce(f32[]{:T(128)S(6)} %add.56), channel_id=1, replica_groups=mesh['fs'=8,'tp'=4] {'tp'}, use_global_device_ids=true, to_apply=%region_2.0 | all-reduce | flops 1 | bytes 8 | tf_op jit(solution)/shard_map/psum | solution.py:50
  90.3 1.2 multiply_add_fusion
  91.5 0.7 copy-done.4
  92.2 2.6 %fusion.23 = (bf16[512,256]{1,0:T(8,128)(2,1)}, f32[512,256]{1,0:T(8,128)}, f32[512,256]{1,0:T(8,128)}) fusion(f32[512,256]{1,0:T(8,128)} %param.19, bf16[2048,128]{1,0:T(8,128)(2,1)} %param.17, s32[]{:T(128)S(6)} %select_n.4, f32[512,128]{0,1:T(8,128)S(1)} %get-tuple-element.27, f32[512,128]{0,1:T(8,128)S(1)} %get-tuple-element.26), kind=kOutput, calls=%fused_computation.35 | convolution fusion | flops 201850880 | bytes 2424836 | tf_op jit(solution)/shard_map/dot_general | solution.py:60
  94.8 0.0 all-gather.5.cloned.1.call-update
  94.8 0.0 all-gather.3.cloned.1.call-start
  94.9 1.2 multiply_add_fusion.2
  96.1 0.7 copy-done.6
  96.8 2.6 %fusion.24 = (bf16[256,512]{1,0:T(8,128)(2,1)}, f32[256,512]{1,0:T(8,128)}, f32[256,512]{1,0:T(8,128)}) fusion(f32[256,512]{1,0:T(8,128)} %param.18, f32[128,512]{1,0:T(8,128)S(1)} %get-tuple-element.48, f32[128,512]{1,0:T(8,128)S(1)} %get-tuple-element.49, bf16[2048,128]{1,0:T(8,128)(2,1)} %param.16, s32[]{:T(128)S(6)} %select_n.4), kind=kOutput, calls=%fused_computation.36 | convolution fusion | flops 201850880 | bytes 2424836 | tf_op jit(solution)/shard_map/dot_general | solution.py:59
  99.4 0.0 all-gather.3.cloned.1.call-update
  99.4 1.8 %copy.25 = f32[512,128]{1,0:T(8,128)} copy(f32[512,128]{0,1:T(8,128)} %copy-done.4) | data formatting | bytes 524288
  101.2 0.8 copy.24
  102.1 20.8 %all-gather.5.cloned.1.call-done = bf16[512,2048]{1,0:T(8,128)(2,1)} async-done(((bf16[512,256]{1,0:T(8,128)(2,1)}), bf16[512,2048]{1,0:T(8,128)(2,1)}) %all-gather.5.cloned.1.call-update) | async-done | bytes 2097168 | tf_op jit(solution)/shard_map/all_gather | solution.py:65
  122.8 30.4 %all-gather.3.cloned.1.call-done = bf16[2048,512]{1,0:T(8,128)(2,1)} async-done(((bf16[256,512]{1,0:T(8,128)(2,1)}), bf16[2048,512]{1,0:T(8,128)(2,1)}) %all-gather.3.cloned.1.call-update) | async-done | bytes 2097168 | tf_op jit(solution)/shard_map/all_gather | solution.py:64
  153.2 3.2 %copy.30 = bf16[2048,512]{1,0:T(8,128)(2,1)} copy(bf16[2048,512]{1,0:T(8,128)(2,1)} %all-gather.3.cloned.1.call-done) | data formatting | bytes 4194304
  156.4 1.3 copy.31
  (16 shorter events, 0.0 us)
Async XLA Ops:
  7.2 1.9 %copy-start = (bf16[768,2048]{1,0:T(8,128)(2,1)S(1)}, bf16[768,2048]{1,0:T(8,128)(2,1)}, u32[]{:S(2)}) copy-start(bf16[768,2048]{1,0:T(8,128)(2,1)} %param.12) | copy-start | bytes 9437188
  7.2 67.5 %all-reduce.3.cloned.1.call-start = ((), (), s32[]{:S(2)}) async-start(), calls=%async_computation.2 | async-start | bytes 1048576 | tf_op jit(solution)/shard_map/psum | solution.py:49
  9.1 2.4 %copy-start.2 = (bf16[768,512]{1,0:T(8,128)(2,1)S(1)}, bf16[768,512]{1,0:T(8,128)(2,1)}, u32[]{:S(2)}) copy-start(bf16[768,512]{1,0:T(8,128)(2,1)} %param.13) | copy-start | bytes 2359300
  9.1 3.6 %copy-start.1 = (bf16[768,2048]{1,0:T(8,128)(2,1)S(1)}, bf16[768,2048]{1,0:T(8,128)(2,1)}, u32[]{:S(2)}) copy-start(bf16[768,2048]{1,0:T(8,128)(2,1)} %param.15) | copy-start | bytes 9437188
  9.1 3.6 %copy-start.8 = (bf16[2048,128]{1,0:T(8,128)(2,1)S(1)}, bf16[2048,128]{1,0:T(8,128)(2,1)}, u32[]{:S(2)}) copy-start(bf16[2048,128]{1,0:T(8,128)(2,1)} %param.17) | copy-start | bytes 1572868
  11.7 2.2 %copy-start.3 = (bf16[768,512]{1,0:T(8,128)(2,1)S(1)}, bf16[768,512]{1,0:T(8,128)(2,1)}, u32[]{:S(2)}) copy-start(bf16[768,512]{1,0:T(8,128)(2,1)} %param.14) | copy-start | bytes 2359300
  12.7 2.5 %copy-start.9 = (f32[512,128]{1,0:T(8,128)S(1)}, f32[512,128]{1,0:T(8,128)}, u32[]{:S(2)}) copy-start(f32[512,128]{1,0:T(8,128)} %param.22) | copy-start | bytes 786436
  15.2 107.7 %all-gather.5.cloned.1.call-start = ((), (), s32[]{:S(2)}) async-start(), calls=%async_computation.1 | async-start | bytes 2359296 | tf_op jit(solution)/shard_map/all_gather | solution.py:65
  91.5 0.7 copy-start.4
  94.8 58.4 %all-gather.3.cloned.1.call-start = ((), (), s32[]{:S(2)}) async-start(), calls=%async_computation | async-start | bytes 2359296 | tf_op jit(solution)/shard_map/all_gather | solution.py:64
  96.1 0.7 copy-start.6
  96.1 3.3 %copy-start.7 = (f32[128,512]{1,0:T(8,128)}, f32[128,512]{1,0:T(8,128)S(1)}, u32[]{:S(2)}) copy-start(f32[128,512]{1,0:T(8,128)S(1)} %get-tuple-element.48) | copy-start | bytes 786436
  153.2 3.2 %copy-start.5 = (bf16[512,2048]{1,0:T(8,128)(2,1)S(1)}, bf16[512,2048]{1,0:T(8,128)(2,1)}, u32[]{:S(2)}) copy-start(bf16[512,2048]{1,0:T(8,128)(2,1)} %all-gather.5.cloned.1.call-done) | copy-start | bytes 6291460
Sparse Core Ops, SparseCore 0:
  15.3 59.3 all-reduce.2
  94.9 27.8 all-gather.4
  125.0 28.1 all-gather.2
where the time goes:
time: 165 us; the launch traced here: 164 us
  waiting for transfers between devices  108 us (65%)
  between operations  15.9 us (10%)
  local copies, waits for them, and re-layouts  13 us (8%)
  matrix products  11.2 us (7%)
  blocking collectives  10.3 us (6%)
  other arithmetic  5.64 us (3%)
    psum x1, waiting for transfers between devices, shards(): low_q, low_o = lax.psum((partial_q, partial_o), 'fs')  56.8 us
    all_gather x1, waiting for transfers between devices, shards(): lax.all_gather(new_weight_q.astype(jnp.bfloat16), 'fs', axis=0, tiled=True)  30.4 us
    all_gather x1, waiting for transfers between devices, shards(): lax.all_gather(new_weight_o.astype(jnp.bfloat16), 'fs', axis=1, tiled=True)  20.8 us
    unnamed x26, local copies, waits for them, and re-layouts  13 us
    psum x1, blocking collectives, shards(): lax.psum((jnp.sum(low_q * low_q), jnp.sum(low_o * low_o)), 'tp')  10.3 us
  transfers between devices with their start and end apart: 3, of which 3 were waited for; matrix products, arithmetic and copies ran while one was open for 6% of the time, Pallas kernels for 0%

commit v1 on v0

v1 whole, which is shorter than its diff:
```python
import functools

import jax
import jax.numpy as jnp
from jax import lax
from jax.experimental import pallas as pl
from jax.experimental.pallas import tpu as pltpu
from jax.sharding import PartitionSpec as P

MESH = pl.DeviceIdType.MESH
BETA_FIRST = 0.9
BETA_SECOND = 0.95
ADAM_EPS = 1e-08
NORM_EPS = 1e-06
CLIP_RMS = 1.0
LEARN_RATE = 0.01
CORES = 2
SCALE = 2.0**33


def split(value):
    upper = value.astype(jnp.bfloat16)
    lower = (value - upper.astype(jnp.float32)).astype(jnp.bfloat16)
    return upper, lower


def encode(weight):
    scaled = weight * SCALE
    square = scaled * scaled
    fourth = square * square
    return jnp.where(weight < 0, -fourth, fourth).astype(jnp.bfloat16)


def decode(code):
    value = code.astype(jnp.float32)
    root = lax.rsqrt(lax.rsqrt(jnp.abs(value))) * (1.0 / SCALE)
    return jnp.where(value < 0, -root, root)


def exchange(
    chips, columns, tile,
    x_hbm, qc_hbm, ho_hbm, oc_hbm, bq_hbm, bo_hbm, wq_hbm, wo_hbm,
    gq, go, low, total,
    xv, qcv, hov, ocv, bqv, bov, part, sib, acc, rs, sums,
    load, load_w, w_send, w_recv, ws_send, ws_recv,
    sib_sem, rs_send, rs_recv, ag_send, ag_recv, as_send, as_recv, tp_send, tp_recv,
):
    me = lax.axis_index("fs")
    tp = lax.axis_index("tp")
    z = me // CORES
    c = lax.rem(me, CORES)
    sibling = me + 1 - 2 * c
    tiles = xv.shape[0] // tile
    piece = acc.shape[1]
    gathered = (gq, go)

    own = [
        pltpu.make_async_copy(wq_hbm, gq.at[me], load_w.at[0]),
        pltpu.make_async_copy(wo_hbm, go.at[me], load_w.at[1]),
    ]
    for copy in own:
        copy.start()
    whole = ((bq_hbm, bqv), (bo_hbm, bov))
    cut = ((x_hbm, xv), (qc_hbm, qcv), (oc_hbm, ocv), (ho_hbm, hov))

    def load_of(k, t):
        source, target = cut[k]
        rows = pl.ds(t * tile, tile)
        return pltpu.make_async_copy(source.at[rows], target.at[rows], load.at[k, t])

    bases = [pltpu.make_async_copy(a, b, load_w.at[2 + i]) for i, (a, b) in enumerate(whole)]
    bases[0].start()
    for k in (0, 1):
        for t in range(tiles):
            load_of(k, t).start()
    bases[1].start()
    for k in (2, 3):
        for t in range(tiles):
            load_of(k, t).start()

    barrier = pltpu.get_barrier_semaphore()
    pl.semaphore_signal(barrier, inc=1, device_id={"fs": sibling}, device_id_type=MESH)
    for d in range(1, chips):
        other = lax.rem(z + d, chips) * CORES + c
        pl.semaphore_signal(barrier, inc=1, device_id={"fs": other}, device_id_type=MESH)
    for d in range(1, columns):
        other = lax.rem(tp + d, columns)
        pl.semaphore_signal(barrier, inc=1, device_id={"tp": other}, device_id_type=MESH)
    pl.semaphore_wait(barrier, 1 + chips - 1 + columns - 1)

    def along(m, b, k, s, target):
        slot = gathered[m].at[b * CORES + c]
        return pltpu.make_async_remote_copy(
            src_ref=slot, dst_ref=slot, send_sem=w_send.at[m, k, s], recv_sem=w_recv.at[m, b],
            device_id={"fs": target}, device_id_type=MESH,
        )

    def across(m, b, core):
        slot = gathered[m].at[b * CORES + core]
        return pltpu.make_async_remote_copy(
            src_ref=slot, dst_ref=slot, send_sem=ws_send.at[m, b], recv_sem=ws_recv.at[m, b],
            device_id={"fs": sibling}, device_id_type=MESH,
        )

    def relay(s, m, first=False):
        for k, sign in ((0, 1), (1, -1)):
            b = z - sign * s
            there = (b >= 0) & (b < chips)
            target = z + sign

            if not first:
                @pl.when(there)
                def _():
                    along(m, b, k, s, me).wait_recv()

            @pl.when(there & (target >= 0) & (target < chips))
            def _():
                along(m, b, k, s, target * CORES + c).start()

            if k == 0 or not first:
                @pl.when(there)
                def _():
                    across(m, b, c).start()

    for m in (0, 1):
        own[m].wait()
        relay(0, m, first=True)

    def multiply(m, basis, wide, narrow):
        def body(t, carry):
            load_of(2 * m, t).wait()
            rows = pl.ds(pl.multiple_of(t * tile, tile), tile)
            thin = jnp.dot(wide[rows, :], basis[...], preferred_element_type=jnp.float32)
            both = jnp.concatenate(split(thin), axis=1)
            load_of(2 * m + 1, t).wait()
            product = lax.dot_general(
                both, narrow[rows, :], (((0,), (0,)), ((), ())), preferred_element_type=jnp.float32
            )
            rank = product.shape[0] // 2
            value = product[:rank] + product[rank:]
            part[m] = value + jnp.where(t > 0, part[m], 0.0)
            return carry

        part[m] = jnp.zeros(part.shape[1:], part.dtype)
        lax.fori_loop(0, tiles, body, 0)

    bases[0].wait()
    multiply(0, bqv, xv, qcv)
    bases[1].wait()
    multiply(1, bov, ocv, hov)

    swap = pltpu.make_async_remote_copy(
        src_ref=part.at[1 - c], dst_ref=sib, send_sem=sib_sem.at[0], recv_sem=sib_sem.at[1],
        device_id={"fs": sibling}, device_id_type=MESH,
    )
    swap.start()
    swap.wait()
    value = part[c] + sib[...]
    for p in range(chips):
        acc[p] = value[p * piece : (p + 1) * piece]

    def scatter(d, source, target):
        return pltpu.make_async_remote_copy(
            src_ref=acc.at[target], dst_ref=rs.at[source], send_sem=rs_send.at[d], recv_sem=rs_recv.at[source],
            device_id={"fs": target * CORES + c}, device_id_type=MESH,
        )

    for d in range(1, chips):
        scatter(d, z, lax.rem(z + d, chips)).start()
    if chips > 1:
        relay(1, 0)
    rs[z] = acc[z]
    for d in range(1, chips):
        source = lax.rem(z + d, chips)
        scatter(d, source, z).wait_recv()
    reduced = rs[0]
    for p in range(1, chips):
        reduced = reduced + rs[p]
    low[c, z] = reduced

    def spread(d, source, target):
        return pltpu.make_async_remote_copy(
            src_ref=low.at[c, source], dst_ref=low.at[c, source], send_sem=ag_send.at[d], recv_sem=ag_recv.at[source],
            device_id={"fs": target * CORES + c}, device_id_type=MESH,
        )

    def hand(p, core):
        return pltpu.make_async_remote_copy(
            src_ref=low.at[core, p], dst_ref=low.at[core, p], send_sem=as_send.at[p], recv_sem=as_recv.at[p],
            device_id={"fs": sibling}, device_id_type=MESH,
        )

    for d in range(1, chips):
        spread(d, z, lax.rem(z + d, chips)).start()
    hand(z, c).start()
    if chips > 1:
        relay(1, 1)
    for d in range(1, chips):
        source = lax.rem(z + d, chips)
        spread(d, source, z).wait_recv()
        hand(source, c).start()
    for p in range(chips):
        hand(p, 1 - c).wait_recv()

    squares = jnp.zeros(acc.shape[1:], jnp.float32)
    for core in range(CORES):
        for p in range(chips):
            entry = low[core, p]
            squares = squares + entry * entry
    sums[tp] = jnp.broadcast_to(jnp.sum(squares, axis=(0, 1), keepdims=True), sums.shape[1:])

    def share(d, source, target):
        return pltpu.make_async_remote_copy(
            src_ref=sums.at[source], dst_ref=sums.at[source], send_sem=tp_send.at[d], recv_sem=tp_recv.at[source],
            device_id={"tp": target}, device_id_type=MESH,
        )

    for d in range(1, columns):
        share(d, tp, lax.rem(tp + d, columns)).start()
    for d in range(1, columns):
        share(d, lax.rem(tp + d, columns), tp).wait_recv()
    everything = sums[0]
    for p in range(1, columns):
        everything = everything + sums[p]
    total[...] = everything

    if chips > 2:
        @pl.loop(2, chips)
        def _(s):
            for m in (0, 1):
                relay(s, m)

    for m in (0, 1):
        for p in range(chips):
            across(m, p, 1 - c).wait_recv()
            across(m, p, c).wait_send()

        @pl.loop(0, chips)
        def _(s):
            for k, sign in ((0, 1), (1, -1)):
                b = z - sign * s
                target = z + sign

                @pl.when((b >= 0) & (b < chips) & (target >= 0) & (target < chips))
                def _():
                    along(m, b, k, s, target * CORES + c).wait_send()

    for d in range(1, chips):
        scatter(d, z, lax.rem(z + d, chips)).wait_send()
        spread(d, z, lax.rem(z + d, chips)).wait_send()
    for p in range(chips):
        hand(p, c).wait_send()
    for d in range(1, columns):
        share(d, tp, lax.rem(tp + d, columns)).wait_send()


def communicate(fs, columns, x, qc, ho, oc, bq, bo, wq, wo):
    chips = fs // CORES
    tokens, width = x.shape
    features = qc.shape[1]
    rank = bq.shape[1]
    piece = rank // chips
    tile = 256 if tokens % 256 == 0 else tokens
    dma = pltpu.SemaphoreType.DMA
    f32 = jnp.float32
    return pl.pallas_call(
        functools.partial(exchange, chips, columns, tile),
        out_shape=(
            jax.ShapeDtypeStruct((fs,) + wq.shape, wq.dtype),
            jax.ShapeDtypeStruct((fs,) + wo.shape, wo.dtype),
            jax.ShapeDtypeStruct((CORES, chips, piece, features), f32),
            jax.ShapeDtypeStruct((8, 128), f32),
        ),
        in_specs=[pl.BlockSpec(memory_space=pl.ANY)] * 8,
        out_specs=[pl.BlockSpec(memory_space=pltpu.VMEM)] * 4,
        scratch_shapes=[
            pltpu.VMEM(x.shape, x.dtype),
            pltpu.VMEM(qc.shape, qc.dtype),
            pltpu.VMEM(ho.shape, ho.dtype),
            pltpu.VMEM(oc.shape, oc.dtype),
            pltpu.VMEM(bq.shape, bq.dtype),
            pltpu.VMEM(bo.shape, bo.dtype),
            pltpu.VMEM((2, rank, features), f32),
            pltpu.VMEM((rank, features), f32),
            pltpu.VMEM((chips, piece, features), f32),
            pltpu.VMEM((chips, piece, features), f32),
            pltpu.VMEM((columns, 8, 128), f32),
            dma((4, tokens // tile)),
            dma((4,)),
            dma((2, 2, chips)),
            dma((2, chips)),
            dma((2, chips)),
            dma((2, chips)),
            dma((2,)),
            dma((chips,)),
            dma((chips,)),
            dma((chips,)),
            dma((chips,)),
            dma((chips,)),
            dma((chips,)),
            dma((columns,)),
            dma((columns,)),
        ],
        compiler_params=pltpu.CompilerParams(
            collective_id=0, has_side_effects=True, vmem_limit_bytes=48 * 1024 * 1024
        ),
        name="exchange",
    )(x, qc, ho, oc, bq, bo, wq, wo)


def shards(
    fs, columns,
    saved_input, query_cot, head_out, output_cot, basis_q, basis_o,
    weight_q, weight_o, first_q, second_q, first_o, second_o,
):
    f32 = jnp.float32
    rank = basis_q.shape[1]
    features = query_cot.shape[1]
    rows = weight_q.shape[0]
    send_q = encode(weight_q)
    send_o = encode(weight_o)
    all_q, all_o, low, total = communicate(
        fs, columns, saved_input, query_cot, head_out, output_cot, basis_q, basis_o, send_q, send_o
    )
    low_q = low[0].reshape(rank, features)
    low_o = low[1].reshape(rank, features).T
    rms_value = jnp.sqrt(total[0, 0] / (2 * rank * features * columns) + NORM_EPS)
    factor = jnp.minimum(1.0, CLIP_RMS / rms_value)
    moment_q = BETA_FIRST * first_q + (1.0 - BETA_FIRST) * factor * low_q
    square_q = BETA_SECOND * second_q + (1.0 - BETA_SECOND) * (factor * low_q) ** 2
    moment_o = BETA_FIRST * first_o + (1.0 - BETA_FIRST) * factor * low_o
    square_o = BETA_SECOND * second_o + (1.0 - BETA_SECOND) * (factor * low_o) ** 2
    dir_q = moment_q / (jnp.sqrt(square_q) + ADAM_EPS)
    dir_o = moment_o / (jnp.sqrt(square_o) + ADAM_EPS)
    upper_q, lower_q = split(dir_q)
    upper_o, lower_o = split(dir_o)

    def steps(bq, bo):
        q = jnp.dot(bq, upper_q, preferred_element_type=f32) + jnp.dot(bq, lower_q, preferred_element_type=f32)
        o = jnp.dot(upper_o, bo.T, preferred_element_type=f32) + jnp.dot(lower_o, bo.T, preferred_element_type=f32)
        return q, o

    offset = lax.axis_index("fs") * rows
    step_q, step_o = steps(
        lax.dynamic_slice_in_dim(basis_q, offset, rows, 0), lax.dynamic_slice_in_dim(basis_o, offset, rows, 0)
    )
    new_weight_q = weight_q - LEARN_RATE * step_q
    new_weight_o = weight_o - LEARN_RATE * step_o
    full_q, full_o = steps(basis_q, basis_o)
    old_q = decode(all_q.reshape(fs * rows, features))
    old_o = decode(all_o.transpose(1, 0, 2).reshape(features, fs * rows))
    copy_q = (old_q - LEARN_RATE * full_q).astype(jnp.bfloat16)
    copy_o = (old_o - LEARN_RATE * full_o).astype(jnp.bfloat16)
    return (
        step_q, step_o, new_weight_q, new_weight_o, copy_q, copy_o,
        moment_q, square_q, moment_o, square_o,
    )


def solution(mesh):
    return jax.shard_map(
        functools.partial(shards, mesh.shape["fs"], mesh.shape["tp"]),
        mesh=mesh,
        in_specs=(
            P("fs", None), P("fs", "tp"), P("fs", "tp"), P("fs", None), P(), P(),
            P("fs", "tp"), P("tp", "fs"), P(None, "tp"), P(None, "tp"), P("tp", None), P("tp", None),
        ),
        out_specs=(
            P("fs", "tp"), P("tp", "fs"), P("fs", "tp"), P("tp", "fs"), P(None, "tp"), P("tp", None),
            P(None, "tp"), P(None, "tp"), P("tp", None), P("tp", None),
        ),
        check_vma=False,
    )
```

time: 165 us -> 120 us (0.73)
  waiting for transfers between devices: 108 us -> 0 us
  Pallas kernels: 0 us -> 56.3 us
  local copies, waits for them, and re-layouts: 13 us -> 36.9 us
  between operations: 15.9 us -> 1.44 us
  blocking collectives: 10.3 us -> 0 us
  other arithmetic: 5.64 us -> 14.7 us
    psum x1 -> x0, waiting for transfers between devices: 56.8 us -> none  [shards(): low_q, low_o = lax.psum((partial_q, partial_o), 'fs')]
    pallas_call x0 -> x1, Pallas kernels: none -> 56.3 us  [communicate(): pl.pallas_call(functools.partial(exchange, chips, columns, tile), out_sha...]
    all_gather x2 -> x0, waiting for transfers between devices: 51.1 us -> none  [the longest x1 30.4 us: shards(): lax.all_gather(new_weight_q.astype(jnp.bfloat16), 'fs', axis=0, tiled=True)]
    mul x0 -> x5, local copies, waits for them, and re-layouts: none -> 19.1 us  [the longest x3 16.5 us: decode(): root = lax.rsqrt(lax.rsqrt(jnp.abs(value))) * (1.0 / SCALE)]
    psum x1 -> x0, blocking collectives: 10.3 us -> none  [shards(): lax.psum((jnp.sum(low_q * low_q), jnp.sum(low_o * low_o)), 'tp')]
    mul x0 -> x3, other arithmetic: none -> 6.96 us  [the longest x2 6.12 us: decode(): root = lax.rsqrt(lax.rsqrt(jnp.abs(value))) * (1.0 / SCALE)]
    lt x0 -> x3, local copies, waits for them, and re-layouts: none -> 5.44 us  [decode(): return jnp.where(value < 0, -root, root)]
    div x0 -> x2, other arithmetic: none -> 4.1 us  [the longest x1 2.09 us: shards(): dir_o = moment_o / (jnp.sqrt(square_o) + ADAM_EPS)]
  transfers between devices with their start and end apart: 3 -> 0, of which waited for: 3 -> 0; matrix products, arithmetic and copies ran while one was open for 6% -> 0% of each run, Pallas kernels for 0% -> 0%
where the time goes in v1:
time: 120 us
  Pallas kernels  56.3 us (47%)
  local copies, waits for them, and re-layouts  36.9 us (31%)
  other arithmetic  14.7 us (12%)
  matrix products  10.2 us (8%)
  between operations  1.44 us (1%)
    pallas_call x1, Pallas kernels, communicate(): pl.pallas_call(functools.partial(exchange, chips, columns, tile), out_sha...  56.3 us
    mul x3, local copies, waits for them, and re-layouts, decode(): root = lax.rsqrt(lax.rsqrt(jnp.abs(value))) * (1.0 / SCALE)  16.5 us
    unnamed x29, local copies, waits for them, and re-layouts  11.8 us
    mul x2, other arithmetic, decode(): root = lax.rsqrt(lax.rsqrt(jnp.abs(value))) * (1.0 / SCALE)  6.12 us
    lt x3, local copies, waits for them, and re-layouts, decode(): return jnp.where(value < 0, -root, root)  5.44 us
    dot_general x2, matrix products, steps(): jnp.dot(lower_o, bo.T, preferred_element_type=f32)  4.73 us
    dot_general x2, matrix products, steps(): jnp.dot(bq, lower_q, preferred_element_type=f32)  3.66 us

profile of v1, /device:TPU:0, one launch (start us, length us, event | category | flops | bytes accessed | tf_op | source)
XLA Modules:
  0.0 119.6 jit_solution(6631592486388136216)
XLA Ops:
  0.6 1.2 fusion.12.wq_hbm
  1.8 1.2 fusion.13.wo_hbm
  3.0 1.0 copy-done
  4.0 1.0 copy-done.2
  5.1 1.1 copy-done.4
  6.2 1.1 copy-done.5
  7.3 56.3 %exchange.1 = (bf16[8,256,512]{2,1,0:T(8,128)(2,1)S(1)}, bf16[8,512,256]{2,1,0:T(8,128)(2,1)}, f32[2,4,32,512]{3,2,1,0:T(8,128)S(1)}, f32[8,128]{1,0:T(8,128)S(1)}) custom-call(bf16[768,2048]{1,0:T(8,128)(2,1)} %x_hbm.1, bf16[768,512]{1,0:T(8,128)(2,1)S(1)} %copy-done.4, bf16[768,512]{1,0:T(8,128)(2,1)S(1)} %copy-done.5, bf16[768,2048]{1,0:T(8,128)(2,1)} %oc_hbm.1, ...), custom_call_target="tpu_custom_call" | custom-call | tf_op jit(solution)/shard_map/exchange/pallas_call | solution.py:266
  63.6 0.5 slice.9
  64.9 0.8 slice_multiply_fusion
  65.7 2.0 %add_divide_fusion.1 = (f32[128,512]{1,0:T(8,128)S(1)}, f32[128,512]{1,0:T(8,128)}, f32[128,512]{1,0:T(8,128)}) fusion(f32[1,4,32,512]{3,2,1,0:T(8,128)S(1)} %get-tuple-element.45, f32[128,512]{1,0:T(8,128)} %param.21, f32[1,4,32,512]{3,2,1,0:T(8,128)S(1)} %get-tuple-element.47, f32[128,512]{1,0:T(8,128)} %param.20), kind=kLoop, calls=%fused_computation.34 | loop fusion | flops 393216 | bytes 1835008 | tf_op jit(solution)/shard_map/div | solution.py:333
  68.4 1.2 multiply_subtract_fusion.1
  69.6 1.8 %copy.29 = f32[128,512]{0,1:T(8,128)} copy(f32[128,512]{1,0:T(8,128)} %bitcast.34) | data formatting | bytes 524288 | tf_op jit(solution)/shard_map/mul | solution.py:332
  71.4 0.8 copy.28
  72.2 2.1 %add_divide_fusion = (f32[512,128]{1,0:T(8,128)S(1)}, f32[512,128]{1,0:T(8,128)}, f32[512,128]{1,0:T(8,128)}) fusion(f32[128,512]{0,1:T(8,128)} %copy.29, f32[512,128]{1,0:T(8,128)} %param.23, f32[128,512]{0,1:T(8,128)} %copy.28, f32[512,128]{1,0:T(8,128)} %param.22), kind=kLoop, calls=%fused_computation.31 | loop fusion | flops 393216 | bytes 1835008 | tf_op jit(solution)/shard_map/div | solution.py:334
  74.5 2.3 %multiply_subtract_fusion = (f32[512,256]{1,0:T(8,128)}, f32[512,256]{1,0:T(8,128)}) fusion(f32[512,256]{1,0:T(8,128)} %param.19, f32[512,256]{1,0:T(8,128)S(1)} %fusion.15, bf16[2048,128]{1,0:T(8,128)(2,1)S(1)} %copy-done.3, s32[]{:T(128)S(6)} %select_n.20, f32[512,128]{1,0:T(8,128)S(1)} %get-tuple-element.38), kind=kOutput, calls=%fused_computation.24 | convolution fusion | flops 34209792 | bytes 2424836 | tf_op jit(solution)/shard_map/dot_general | solution.py:340
  76.8 0.7 convert_compare_fusion.1
  77.5 2.1 %copy.31 = pred[2048,512]{0,1:T(32,128)(4,1)} copy(pred[2048,512]{1,0:T(32,128)(4,1)S(1)} %bitcast.31) | data formatting | bytes 2097152 | tf_op jit(solution)/shard_map/lt | solution.py:37
  79.6 3.0 %fusion.2 = f32[8,256,512]{2,1,0:T(8,128)} fusion(bf16[8,256,512]{2,1,0:T(8,128)(2,1)S(1)} %get-tuple-element.16), kind=kLoop, calls=%fused_computation.8 | loop fusion | flops 3145728 | bytes 6291456 | tf_op jit(solution)/shard_map/mul | solution.py:36
  82.7 5.6 %copy.30 = f32[2048,512]{0,1:T(8,128)} copy(f32[2048,512]{1,0:T(8,128)} %bitcast.29) | data formatting | bytes 8388608 | tf_op jit(solution)/shard_map/mul | solution.py:36
  88.3 0.7 fusion.27
  89.0 1.4 %copy-done.6 = f32[2048,512]{0,1:T(8,128)S(1)} copy-done((f32[2048,512]{0,1:T(8,128)S(1)}, f32[2048,512]{0,1:T(8,128)}, u32[]{:S(2)}) %copy-start.6) | copy-done | bytes 4194328
  90.4 2.5 %fusion.8 = bf16[2048,512]{0,1:T(8,128)(2,1)} fusion(pred[2048,512]{0,1:T(32,128)(4,1)S(1)} %copy-done.12, f32[2048,512]{0,1:T(8,128)S(1)} %copy-done.6, f32[512,2048]{1,0:T(8,128)S(1)} %fusion.27, bf16[2048,128]{1,0:T(8,128)(2,1)S(1)} %copy-done.1, f32[128,512]{1,0:T(8,128)S(1)} %copy-done.10), kind=kOutput, calls=%fused_computation.14 | convolution fusion | flops 274989056 | bytes 12320768 | tf_op jit(solution)/shard_map/dot_general | solution.py:339
  92.9 4.1 %copy.38 = bf16[2048,512]{1,0:T(8,128)(2,1)} copy(bf16[2048,512]{0,1:T(8,128)(2,1)} %fusion.8) | data formatting | bytes 4194304
  97.0 0.7 fusion.11
  97.7 1.2 copy.33
  98.8 2.1 %copy.36 = pred[512,2048]{1,0:T(32,128)(4,1)} copy(pred[512,2048]{0,1:T(32,128)(4,1)S(1)} %bitcast.32) | data formatting | bytes 2097152 | tf_op jit(solution)/shard_map/lt | solution.py:37
  101.0 3.1 %fusion.6 = f32[512,8,256]{2,0,1:T(8,128)} fusion(bf16[8,512,256]{2,1,0:T(8,128)(2,1)S(1)} %copy-done.8), kind=kLoop, calls=%fused_computation.12 | loop fusion | flops 3145728 | bytes 6291456 | tf_op jit(solution)/shard_map/mul | solution.py:36
  104.0 5.4 %copy.34 = f32[512,8,256]{0,2,1:T(8,128)} copy(f32[512,8,256]{2,0,1:T(8,128)} %fusion.6) | data formatting | bytes 8388608 | tf_op jit(solution)/shard_map/mul | solution.py:36
  109.4 5.6 %copy.35 = f32[512,2048]{1,0:T(8,128)} copy(f32[512,2048]{0,1:T(8,128)} %bitcast.30) | data formatting | bytes 8388608 | tf_op jit(solution)/shard_map/mul | solution.py:36
  115.0 0.7 fusion.24
  115.7 1.5 %copy-done.7 = f32[512,2048]{1,0:T(8,128)S(1)} copy-done((f32[512,2048]{1,0:T(8,128)S(1)}, f32[512,2048]{1,0:T(8,128)}, u32[]{:S(2)}) %copy-start.7) | copy-done | bytes 4194328
  117.2 2.5 %fusion.10 = bf16[512,2048]{1,0:T(8,128)(2,1)} fusion(pred[512,2048]{1,0:T(32,128)(4,1)S(1)} %copy-done.11, f32[512,2048]{1,0:T(8,128)S(1)} %copy-done.7, f32[512,2048]{1,0:T(8,128)S(1)} %fusion.24, bf16[2048,128]{1,0:T(8,128)(2,1)S(1)} %copy-done.3, f32[512,128]{1,0:T(8,128)S(1)} %get-tuple-element.38), kind=kOutput, calls=%fused_computation.16 | convolution fusion | flops 274989056 | bytes 12320768 | tf_op jit(solution)/shard_map/dot_general | solution.py:340
  (24 shorter events, 1.0 us)
Async XLA Ops:
  3.0 1.0 copy-start
  4.0 1.0 copy-start.2
  5.1 1.1 copy-start.4
  6.2 1.1 copy-start.5
  7.3 60.4 %copy-start.1 = (bf16[2048,128]{1,0:T(8,128)(2,1)S(1)}, bf16[2048,128]{1,0:T(8,128)(2,1)}, u32[]{:S(2)}) copy-start(bf16[2048,128]{1,0:T(8,128)(2,1)} %bq_hbm.1) | copy-start | bytes 1572868
  64.9 3.6 %copy-start.13 = (f32[256,512]{1,0:T(8,128)S(1)}, f32[256,512]{1,0:T(8,128)}, u32[]{:S(2)}) copy-start(f32[256,512]{1,0:T(8,128)} %param.18) | copy-start | bytes 1572868
  65.7 8.6 %copy-start.3 = (bf16[2048,128]{1,0:T(8,128)(2,1)S(1)}, bf16[2048,128]{1,0:T(8,128)(2,1)}, u32[]{:S(2)}) copy-start(bf16[2048,128]{1,0:T(8,128)(2,1)} %bo_hbm.1) | copy-start | bytes 1572868
  67.7 0.7 copy-start.9
  82.7 5.6 %copy-start.10 = (f32[128,512]{1,0:T(8,128)S(1)}, f32[128,512]{1,0:T(8,128)}, u32[]{:S(2)}) copy-start(f32[128,512]{1,0:T(8,128)} %copy-done.9) | copy-start | bytes 786436
  82.7 6.3 %copy-start.12 = (pred[2048,512]{0,1:T(32,128)(4,1)S(1)}, pred[2048,512]{0,1:T(32,128)(4,1)}, u32[]{:S(2)}) copy-start(pred[2048,512]{0,1:T(32,128)(4,1)} %copy.31) | copy-start | bytes 3145732
  88.2 2.2 %copy-start.6 = (f32[2048,512]{0,1:T(8,128)S(1)}, f32[2048,512]{0,1:T(8,128)}, u32[]{:S(2)}) copy-start(f32[2048,512]{0,1:T(8,128)} %copy.30) | copy-start | bytes 12582916
  92.9 4.1 %copy-start.8 = (bf16[8,512,256]{2,1,0:T(8,128)(2,1)S(1)}, bf16[8,512,256]{2,1,0:T(8,128)(2,1)}, u32[]{:S(2)}) copy-start(bf16[8,512,256]{2,1,0:T(8,128)(2,1)} %get-tuple-element.17) | copy-start | bytes 6291460
  109.4 6.3 %copy-start.11 = (pred[512,2048]{1,0:T(32,128)(4,1)S(1)}, pred[512,2048]{1,0:T(32,128)(4,1)}, u32[]{:S(2)}) copy-start(pred[512,2048]{1,0:T(32,128)(4,1)} %copy.36) | copy-start | bytes 3145732
  115.0 2.2 %copy-start.7 = (f32[512,2048]{1,0:T(8,128)S(1)}, f32[512,2048]{1,0:T(8,128)}, u32[]{:S(2)}) copy-start(f32[512,2048]{1,0:T(8,128)} %copy.35) | copy-start | bytes 12582916

commit v2 on v1

--- a/solution.py
+++ b/solution.py
@@ -308,52 +308,115 @@
     )(x, qc, ho, oc, bq, bo, wq, wo)
 
 
+def adam(low, first, second, factor):
+    scaled = factor * low
+    moment = BETA_FIRST * first + (1.0 - BETA_FIRST) * scaled
+    square = BETA_SECOND * second + (1.0 - BETA_SECOND) * (scaled * scaled)
+    return moment, square, moment / (jnp.sqrt(square) + ADAM_EPS)
+
+
+def finish(fs, count, *refs):
+    gq, go, low, total, bq, bo, wq, wo, fq, sq, fo, so = refs[:12]
+    outs, made, sem = refs[12:22], refs[22:32], refs[32]
+    step_q, step_o, new_q, new_o, copy_q, copy_o, moment_q, square_q, moment_o, square_o = made
+    f32 = jnp.float32
+    me = lax.axis_index("fs")
+    rows = wq.shape[0]
+    features = wo.shape[0]
+    started = []
+
+    def write(i, part=None, index=0):
+        source, target = made[i], outs[i]
+        if part is not None:
+            source, target = source.at[part], target.at[part]
+        copy = pltpu.make_async_copy(source, target, sem.at[i, index])
+        copy.start()
+        started.append(copy)
+
+    factor = jnp.minimum(1.0, CLIP_RMS / jnp.sqrt(total[0:1, 0:1] * (1.0 / count) + NORM_EPS))
+    low_q = jnp.concatenate([low[0, p] for p in range(low.shape[1])], axis=0)
+    moment_q[...], square_q[...], dir_q = adam(low_q, fq[...], sq[...], factor)
+    write(6)
+    write(7)
+    low_o = jnp.concatenate([low[1, p] for p in range(low.shape[1])], axis=0).T
+    moment_o[...], square_o[...], dir_o = adam(low_o, fo[...], so[...], factor)
+    write(8)
+    write(9)
+    pair_q = jnp.concatenate(split(dir_q), axis=0)
+    pair_o = jnp.concatenate(split(dir_o), axis=1)
+
+    def make_q(part):
+        basis = bq[part, :]
+        return jnp.dot(jnp.concatenate([basis, basis], axis=1), pair_q, preferred_element_type=f32)
+
+    def make_o(left, part):
+        basis = bo[part, :]
+        both = jnp.concatenate([basis, basis], axis=1)
+        return lax.dot_general(left, both, (((1,), (1,)), ((), ())), preferred_element_type=f32)
+
+    mine = pl.ds(pl.multiple_of(me * rows, rows), rows)
+    step = make_q(mine)
+    step_q[...] = step
+    new_q[...] = wq[...] - LEARN_RATE * step
+    write(0)
+    write(2)
+    step = make_o(pair_o, mine)
+    step_o[...] = step
+    new_o[...] = wo[...] - LEARN_RATE * step
+    write(1)
+    write(3)
+
+    for j in range(fs):
+        part = pl.ds(j * rows, rows)
+        copy_q[part, :] = (decode(gq[j]) - LEARN_RATE * make_q(part)).astype(copy_q.dtype)
+        write(4, part, j)
+    tall = 128
+    for r in range(features // tall):
+        part = pl.ds(r * tall, tall)
+        left = pair_o[r * tall : (r + 1) * tall]
+        for j in range(fs):
+            columns = pl.ds(j * rows, rows)
+            value = decode(go[j, part, :]) - LEARN_RATE * make_o(left, columns)
+            copy_o[part, columns] = value.astype(copy_o.dtype)
+        write(5, part, r)
+    for copy in started:
+        copy.wait()
+
+
+def update(fs, columns, gq, go, low, total, bq, bo, wq, wo, fq, sq, fo, so):
+    f32 = jnp.float32
+    rank, features = fq.shape
+    rows = wq.shape[0]
+    width = fs * rows
+    outs = (
+        (wq.shape, f32), (wo.shape, f32), (wq.shape, f32), (wo.shape, f32),
+        ((width, features), jnp.bfloat16), ((features, width), jnp.bfloat16),
+        (fq.shape, f32), (fq.shape, f32), (fo.shape, f32), (fo.shape, f32),
+    )
+    return pl.pallas_call(
+        functools.partial(finish, fs, 2 * rank * features * columns),
+        out_shape=tuple(jax.ShapeDtypeStruct(*out) for out in outs),
+        in_specs=[pl.BlockSpec(memory_space=pltpu.VMEM)] * 12,
+        out_specs=[pl.BlockSpec(memory_space=pl.ANY)] * 10,
+        scratch_shapes=[pltpu.VMEM(*out) for out in outs] + [pltpu.SemaphoreType.DMA((10, max(fs, features // 128)))],
+        compiler_params=pltpu.CompilerParams(vmem_limit_bytes=48 * 1024 * 1024),
+        name="update",
+    )(gq, go, low, total, bq, bo, wq, wo, fq, sq, fo, so)
+
+
 def shards(
     fs, columns,
     saved_input, query_cot, head_out, output_cot, basis_q, basis_o,
     weight_q, weight_o, first_q, second_q, first_o, second_o,
 ):
-    f32 = jnp.float32
-    rank = basis_q.shape[1]
-    features = query_cot.shape[1]
-    rows = weight_q.shape[0]
     send_q = encode(weight_q)
     send_o = encode(weight_o)
     all_q, all_o, low, total = communicate(
         fs, columns, saved_input, query_cot, head_out, output_cot, basis_q, basis_o, send_q, send_o
     )
-    low_q = low[0].reshape(rank, features)
-    low_o = low[1].reshape(rank, features).T
-    rms_value = jnp.sqrt(total[0, 0] / (2 * rank * features * columns) + NORM_EPS)
-    factor = jnp.minimum(1.0, CLIP_RMS / rms_value)
-    moment_q = BETA_FIRST * first_q + (1.0 - BETA_FIRST) * factor * low_q
-    square_q = BETA_SECOND * second_q + (1.0 - BETA_SECOND) * (factor * low_q) ** 2
-    moment_o = BETA_FIRST * first_o + (1.0 - BETA_FIRST) * factor * low_o
-    square_o = BETA_SECOND * second_o + (1.0 - BETA_SECOND) * (factor * low_o) ** 2
-    dir_q = moment_q / (jnp.sqrt(square_q) + ADAM_EPS)
-    dir_o = moment_o / (jnp.sqrt(square_o) + ADAM_EPS)
-    upper_q, lower_q = split(dir_q)
-    upper_o, lower_o = split(dir_o)
-
-    def steps(bq, bo):
-        q = jnp.dot(bq, upper_q, preferred_element_type=f32) + jnp.dot(bq, lower_q, preferred_element_type=f32)
-        o = jnp.dot(upper_o, bo.T, preferred_element_type=f32) + jnp.dot(lower_o, bo.T, preferred_element_type=f32)
-        return q, o
-
-    offset = lax.axis_index("fs") * rows
-    step_q, step_o = steps(
-        lax.dynamic_slice_in_dim(basis_q, offset, rows, 0), lax.dynamic_slice_in_dim(basis_o, offset, rows, 0)
-    )
-    new_weight_q = weight_q - LEARN_RATE * step_q
-    new_weight_o = weight_o - LEARN_RATE * step_o
-    full_q, full_o = steps(basis_q, basis_o)
-    old_q = decode(all_q.reshape(fs * rows, features))
-    old_o = decode(all_o.transpose(1, 0, 2).reshape(features, fs * rows))
-    copy_q = (old_q - LEARN_RATE * full_q).astype(jnp.bfloat16)
-    copy_o = (old_o - LEARN_RATE * full_o).astype(jnp.bfloat16)
-    return (
-        step_q, step_o, new_weight_q, new_weight_o, copy_q, copy_o,
-        moment_q, square_q, moment_o, square_o,
+    return update(
+        fs, columns, all_q, all_o, low, total, basis_q, basis_o,
+        weight_q, weight_o, first_q, second_q, first_o, second_o,
     )
 
 

time: 120 us -> 69 us (0.57)
  local copies, waits for them, and re-layouts: 36.9 us -> 2.11 us
  other arithmetic: 14.7 us -> 2.43 us
  matrix products: 10.2 us -> 0 us
  Pallas kernels: 56.3 us -> 63.4 us
    mul x5 -> x0, local copies, waits for them, and re-layouts: 19.1 us -> none  [the longest x3 16.5 us: decode(): root = lax.rsqrt(lax.rsqrt(jnp.abs(value))) * (1.0 / SCALE)]
    dot_general x8 -> x0, matrix products: 10.2 us -> none  [the longest x2 4.73 us: steps(): jnp.dot(lower_o, bo.T, preferred_element_type=f32)]
    unnamed x29 -> x20, local copies, waits for them, and re-layouts: 11.8 us -> 2.11 us
    pallas_call x0 -> x1, Pallas kernels: none -> 7.09 us  [update(): pl.pallas_call(functools.partial(finish, fs, 2 * rank * features * column...]
    mul x3 -> x0, other arithmetic: 6.96 us -> none  [the longest x2 6.12 us: decode(): root = lax.rsqrt(lax.rsqrt(jnp.abs(value))) * (1.0 / SCALE)]
    lt x3 -> x0, local copies, waits for them, and re-layouts: 5.44 us -> none  [decode(): return jnp.where(value < 0, -root, root)]
    div x2 -> x0, other arithmetic: 4.1 us -> none  [the longest x1 2.09 us: shards(): dir_o = moment_o / (jnp.sqrt(square_o) + ADAM_EPS)]
    lt x2 -> x0, other arithmetic: 1.36 us -> none  [decode(): return jnp.where(value < 0, -root, root)]
where the time goes in v2:
time: 69 us; the launch traced here: 68.7 us
  Pallas kernels  63.4 us (92%)
  other arithmetic  2.43 us (4%)
  local copies, waits for them, and re-layouts  2.11 us (3%)
  between operations  0.76 us (1%)
    pallas_call x1, Pallas kernels, communicate(): pl.pallas_call(functools.partial(exchange, chips, columns, tile), out_sha...  56.3 us
    pallas_call x1, Pallas kernels, update(): pl.pallas_call(functools.partial(finish, fs, 2 * rank * features * column...  7.09 us
    convert_element_type x2, other arithmetic, encode(): return jnp.where(weight < 0, -fourth, fourth).astype(jnp.bfloat16)  2.43 us
    unnamed x20, local copies, waits for them, and re-layouts  2.11 us

profile of v2, /device:TPU:0, one launch (start us, length us, event | category | flops | bytes accessed | tf_op | source)
XLA Modules:
  0.0 68.7 jit_solution(1539048217122893348)
XLA Ops:
  0.6 0.0 copy-start.5
  0.7 0.0 copy-start.4
  0.7 1.3 %fusion.wq_hbm = bf16[256,512]{1,0:T(8,128)(2,1)S(1)} fusion(f32[256,512]{1,0:T(8,128)} %refs_6_.1), kind=kLoop, calls=%fused_computation.2 | loop fusion | flops 917504 | bytes 786432 | tf_op jit(solution)/shard_map/convert_element_type | solution.py:31
  1.9 1.2 %fusion.1.wo_hbm = bf16[512,256]{1,0:T(8,128)(2,1)S(1)} fusion(f32[512,256]{1,0:T(8,128)} %refs_7_.1), kind=kLoop, calls=%fused_computation.3 | loop fusion | flops 917504 | bytes 786432 | tf_op jit(solution)/shard_map/convert_element_type | solution.py:31
  3.1 0.0 copy-done.5
  3.1 0.0 copy-done.4
  3.1 0.0 copy-start
  3.1 1.0 %copy-done = bf16[2048,128]{1,0:T(8,128)(2,1)S(1)} copy-done((bf16[2048,128]{1,0:T(8,128)(2,1)S(1)}, bf16[2048,128]{1,0:T(8,128)(2,1)}, u32[]{:S(2)}) %copy-start) | copy-done | bytes 524312
  4.2 0.0 copy-start.1
  4.2 1.0 %copy-done.1 = bf16[2048,128]{1,0:T(8,128)(2,1)S(1)} copy-done((bf16[2048,128]{1,0:T(8,128)(2,1)S(1)}, bf16[2048,128]{1,0:T(8,128)(2,1)}, u32[]{:S(2)}) %copy-start.1) | copy-done | bytes 524312
  5.2 0.0 copy-start.2
  5.2 0.0 copy-start.3
  5.2 0.0 copy-start.6
  5.2 0.0 copy-start.7
  5.2 0.0 copy-start.8
  5.2 0.0 copy-start.9
  5.2 56.3 %exchange.1 = (bf16[8,256,512]{2,1,0:T(8,128)(2,1)S(1)}, bf16[8,512,256]{2,1,0:T(8,128)(2,1)}, f32[2,4,32,512]{3,2,1,0:T(8,128)S(1)}, f32[8,128]{1,0:T(8,128)S(1)}) custom-call(bf16[768,2048]{1,0:T(8,128)(2,1)} %x_hbm.1, bf16[768,512]{1,0:T(8,128)(2,1)S(1)} %copy-done.4, bf16[768,512]{1,0:T(8,128)(2,1)S(1)} %copy-done.5, bf16[768,2048]{1,0:T(8,128)(2,1)} %oc_hbm.1, ...), custom_call_target="tpu_custom_call" | custom-call | tf_op jit(solution)/shard_map/exchange/pallas_call | solution.py:266
  61.6 0.0 copy-done.2
  61.6 0.0 copy-done.3
  61.6 0.0 copy-done.6
  61.6 0.0 copy-done.7
  61.6 0.0 copy-done.8
  61.6 0.0 copy-done.9
  61.6 7.1 %update.1 = (f32[256,512]{1,0:T(8,128)}, f32[512,256]{1,0:T(8,128)}, f32[256,512]{1,0:T(8,128)}, f32[512,256]{1,0:T(8,128)}, bf16[2048,512]{1,0:T(8,128)(2,1)}, ...) custom-call(bf16[8,256,512]{2,1,0:T(8,128)(2,1)S(1)} %get-tuple-elem, ...), custom_call_target="tpu_custom_call" | custom-call | tf_op jit(solution)/shard_map/update/pallas_call | solution.py:396
Async XLA Ops:
  0.6 2.5 %copy-start.5 = (bf16[768,512]{1,0:T(8,128)(2,1)S(1)}, bf16[768,512]{1,0:T(8,128)(2,1)}, u32[]{:S(2)}) copy-start(bf16[768,512]{1,0:T(8,128)(2,1)} %ho_hbm.1) | copy-start | bytes 2359300
  0.7 2.5 %copy-start.4 = (bf16[768,512]{1,0:T(8,128)(2,1)S(1)}, bf16[768,512]{1,0:T(8,128)(2,1)}, u32[]{:S(2)}) copy-start(bf16[768,512]{1,0:T(8,128)(2,1)} %qc_hbm.1) | copy-start | bytes 2359300
  3.1 1.0 %copy-start = (bf16[2048,128]{1,0:T(8,128)(2,1)S(1)}, bf16[2048,128]{1,0:T(8,128)(2,1)}, u32[]{:S(2)}) copy-start(bf16[2048,128]{1,0:T(8,128)(2,1)} %refs_4_.1) | copy-start | bytes 1572868
  4.2 1.0 %copy-start.1 = (bf16[2048,128]{1,0:T(8,128)(2,1)S(1)}, bf16[2048,128]{1,0:T(8,128)(2,1)}, u32[]{:S(2)}) copy-start(bf16[2048,128]{1,0:T(8,128)(2,1)} %refs_5_.1) | copy-start | bytes 1572868
  5.2 56.4 %copy-start.2 = (f32[256,512]{1,0:T(8,128)S(1)}, f32[256,512]{1,0:T(8,128)}, u32[]{:S(2)}) copy-start(f32[256,512]{1,0:T(8,128)} %refs_6_.1) | copy-start | bytes 1572868
  5.2 56.4 %copy-start.3 = (f32[512,256]{1,0:T(8,128)S(1)}, f32[512,256]{1,0:T(8,128)}, u32[]{:S(2)}) copy-start(f32[512,256]{1,0:T(8,128)} %refs_7_.1) | copy-start | bytes 1572868
  5.2 56.4 %copy-start.6 = (f32[128,512]{1,0:T(8,128)S(1)}, f32[128,512]{1,0:T(8,128)}, u32[]{:S(2)}) copy-start(f32[128,512]{1,0:T(8,128)} %refs_8_.1) | copy-start | bytes 786436
  5.2 56.4 %copy-start.7 = (f32[128,512]{1,0:T(8,128)S(1)}, f32[128,512]{1,0:T(8,128)}, u32[]{:S(2)}) copy-start(f32[128,512]{1,0:T(8,128)} %refs_9_.1) | copy-start | bytes 786436
  5.2 56.4 %copy-start.8 = (f32[512,128]{1,0:T(8,128)S(1)}, f32[512,128]{1,0:T(8,128)}, u32[]{:S(2)}) copy-start(f32[512,128]{1,0:T(8,128)} %refs_10_.1) | copy-start | bytes 786436
  5.2 56.4 %copy-start.9 = (f32[512,128]{1,0:T(8,128)S(1)}, f32[512,128]{1,0:T(8,128)}, u32[]{:S(2)}) copy-start(f32[512,128]{1,0:T(8,128)} %refs_11_.1) | copy-start | bytes 786436

commit v3 on v2

--- a/solution.py
+++ b/solution.py
@@ -41,7 +41,7 @@
     chips, columns, tile,
     x_hbm, qc_hbm, ho_hbm, oc_hbm, bq_hbm, bo_hbm, wq_hbm, wo_hbm,
     gq, go, low, total,
-    xv, qcv, hov, ocv, bqv, bov, part, sib, acc, rs, sums,
+    xv, qcv, hov, ocv, bqv, bov, wqv, wov, part, sib, acc, rs, sums,
     load, load_w, w_send, w_recv, ws_send, ws_recv,
     sib_sem, rs_send, rs_recv, ag_send, ag_recv, as_send, as_recv, tp_send, tp_recv,
 ):
@@ -55,8 +55,8 @@
     gathered = (gq, go)
 
     own = [
-        pltpu.make_async_copy(wq_hbm, gq.at[me], load_w.at[0]),
-        pltpu.make_async_copy(wo_hbm, go.at[me], load_w.at[1]),
+        pltpu.make_async_copy(wq_hbm, wqv, load_w.at[0]),
+        pltpu.make_async_copy(wo_hbm, wov, load_w.at[1]),
     ]
     for copy in own:
         copy.start()
@@ -86,6 +86,9 @@
     for d in range(1, columns):
         other = lax.rem(tp + d, columns)
         pl.semaphore_signal(barrier, inc=1, device_id={"tp": other}, device_id_type=MESH)
+    for m, weight in enumerate((wqv, wov)):
+        own[m].wait()
+        gathered[m][me] = encode(weight[...])
     pl.semaphore_wait(barrier, 1 + chips - 1 + columns - 1)
 
     def along(m, b, k, s, target):
@@ -123,7 +126,6 @@
                     across(m, b, c).start()
 
     for m in (0, 1):
-        own[m].wait()
         relay(0, m, first=True)
 
     def multiply(m, basis, wide, narrow):
@@ -148,6 +150,8 @@
     multiply(0, bqv, xv, qcv)
     bases[1].wait()
     multiply(1, bov, ocv, hov)
+    if chips > 1:
+        relay(1, 0)
 
     swap = pltpu.make_async_remote_copy(
         src_ref=part.at[1 - c], dst_ref=sib, send_sem=sib_sem.at[0], recv_sem=sib_sem.at[1],
@@ -168,7 +172,7 @@
     for d in range(1, chips):
         scatter(d, z, lax.rem(z + d, chips)).start()
     if chips > 1:
-        relay(1, 0)
+        relay(1, 1)
     rs[z] = acc[z]
     for d in range(1, chips):
         source = lax.rem(z + d, chips)
@@ -193,8 +197,9 @@
     for d in range(1, chips):
         spread(d, z, lax.rem(z + d, chips)).start()
     hand(z, c).start()
-    if chips > 1:
-        relay(1, 1)
+    if chips > 2:
+        relay(2, 0)
+        relay(2, 1)
     for d in range(1, chips):
         source = lax.rem(z + d, chips)
         spread(d, source, z).wait_recv()
@@ -224,8 +229,8 @@
         everything = everything + sums[p]
     total[...] = everything
 
-    if chips > 2:
-        @pl.loop(2, chips)
+    if chips > 3:
+        @pl.loop(3, chips)
         def _(s):
             for m in (0, 1):
                 relay(s, m)
@@ -266,12 +271,12 @@
     return pl.pallas_call(
         functools.partial(exchange, chips, columns, tile),
         out_shape=(
-            jax.ShapeDtypeStruct((fs,) + wq.shape, wq.dtype),
-            jax.ShapeDtypeStruct((fs,) + wo.shape, wo.dtype),
+            jax.ShapeDtypeStruct((fs,) + wq.shape, jnp.bfloat16),
+            jax.ShapeDtypeStruct((fs,) + wo.shape, jnp.bfloat16),
             jax.ShapeDtypeStruct((CORES, chips, piece, features), f32),
             jax.ShapeDtypeStruct((8, 128), f32),
         ),
-        in_specs=[pl.BlockSpec(memory_space=pl.ANY)] * 8,
+        in_specs=[pl.BlockSpec(memory_space=pltpu.HBM)] * 8,
         out_specs=[pl.BlockSpec(memory_space=pltpu.VMEM)] * 4,
         scratch_shapes=[
             pltpu.VMEM(x.shape, x.dtype),
@@ -280,6 +285,8 @@
             pltpu.VMEM(oc.shape, oc.dtype),
             pltpu.VMEM(bq.shape, bq.dtype),
             pltpu.VMEM(bo.shape, bo.dtype),
+            pltpu.VMEM(wq.shape, wq.dtype),
+            pltpu.VMEM(wo.shape, wo.dtype),
             pltpu.VMEM((2, rank, features), f32),
             pltpu.VMEM((rank, features), f32),
             pltpu.VMEM((chips, piece, features), f32),
@@ -302,7 +309,7 @@
             dma((columns,)),
         ],
         compiler_params=pltpu.CompilerParams(
-            collective_id=0, has_side_effects=True, vmem_limit_bytes=48 * 1024 * 1024
+            collective_id=0, has_side_effects=True, vmem_limit_bytes=63 * 1024 * 1024
         ),
         name="exchange",
     )(x, qc, ho, oc, bq, bo, wq, wo)
@@ -399,7 +406,7 @@
         in_specs=[pl.BlockSpec(memory_space=pltpu.VMEM)] * 12,
         out_specs=[pl.BlockSpec(memory_space=pl.ANY)] * 10,
         scratch_shapes=[pltpu.VMEM(*out) for out in outs] + [pltpu.SemaphoreType.DMA((10, max(fs, features // 128)))],
-        compiler_params=pltpu.CompilerParams(vmem_limit_bytes=48 * 1024 * 1024),
+        compiler_params=pltpu.CompilerParams(vmem_limit_bytes=63 * 1024 * 1024),
         name="update",
     )(gq, go, low, total, bq, bo, wq, wo, fq, sq, fo, so)
 
@@ -409,10 +416,8 @@
     saved_input, query_cot, head_out, output_cot, basis_q, basis_o,
     weight_q, weight_o, first_q, second_q, first_o, second_o,
 ):
-    send_q = encode(weight_q)
-    send_o = encode(weight_o)
     all_q, all_o, low, total = communicate(
-        fs, columns, saved_input, query_cot, head_out, output_cot, basis_q, basis_o, send_q, send_o
+        fs, columns, saved_input, query_cot, head_out, output_cot, basis_q, basis_o, weight_q, weight_o
     )
     return update(
         fs, columns, all_q, all_o, low, total, basis_q, basis_o,

time: 69 us -> 62.9 us (0.912)
  other arithmetic: 2.43 us -> 0 us
  local copies, waits for them, and re-layouts: 2.11 us -> 0 us
  Pallas kernels: 63.4 us -> 62.1 us
    pallas_call x1, Pallas kernels: 56.3 us -> 53.5 us  [communicate(): pl.pallas_call(functools.partial(exchange, chips, columns, tile), out_sha...]
    convert_element_type x2 -> x0, other arithmetic: 2.43 us -> none  [encode(): return jnp.where(weight < 0, -fourth, fourth).astype(jnp.bfloat16)]
    unnamed x20 -> x0, local copies, waits for them, and re-layouts: 2.11 us -> none
    pallas_call x1, Pallas kernels: 7.09 us -> 8.66 us  [update(): pl.pallas_call(functools.partial(finish, fs, 2 * rank * features * column...]
where the time goes in v3:
time: 62.9 us; the launch traced here: 62.8 us
  Pallas kernels  62.1 us (99%)
  between operations  0.65 us (1%)
    pallas_call x1, Pallas kernels, communicate(): pl.pallas_call(functools.partial(exchange, chips, columns, tile), out_sha...  53.5 us
    pallas_call x1, Pallas kernels, update(): pl.pallas_call(functools.partial(finish, fs, 2 * rank * features * column...  8.66 us

profile of v3, /device:TPU:0, one launch (start us, length us, event | category | flops | bytes accessed | tf_op | source)
XLA Modules:
  0.0 62.8 jit_solution(18165974286462486915)
XLA Ops:
  0.6 53.5 %exchange.1 = (bf16[8,256,512]{2,1,0:T(8,128)(2,1)}, bf16[8,512,256]{2,1,0:T(8,128)(2,1)}, f32[2,4,32,512]{3,2,1,0:T(8,128)}, f32[8,128]{1,0:T(8,128)}) custom-call(bf16[768,2048]{1,0:T(8,128)(2,1)} %x_hbm.1, bf16[768,512]{1,0:T(8,128)(2,1)} %qc_hbm.1, bf16[768,512]{1,0:T(8,128)(2,1)} %ho_hbm.1, bf16[768,2048]{1,0:T(8,128)(2,1)} %oc_hbm.1, ...), custom_call_target="tpu_custom_call" | custom-call | tf_op jit(solution)/shard_map/exchange/pallas_call | solution.py:271
  54.1 8.7 %update.1 = (f32[256,512]{1,0:T(8,128)}, f32[512,256]{1,0:T(8,128)}, f32[256,512]{1,0:T(8,128)}, f32[512,256]{1,0:T(8,128)}, bf16[2048,512]{1,0:T(8,128)(2,1)}, ...) custom-call(bf16[8,256,512]{2,1,0:T(8,128)(2,1)} %get-tuple-element., ...), custom_call_target="tpu_custom_call" | custom-call | tf_op jit(solution)/shard_map/update/pallas_call | solution.py:403
